TPU v7x, 32 devices: a whole 2x2x4 slice. The times are simulated.
32 devices in a mesh: gr: 2 (over x), fs: 4 (over z), tp: 4 (over y, core).
Axes of the slice: x: 2, y: 2, z: 4, core: 2. Of those that a mesh axis runs over, the one named last changes fastest.
Arguments:
- tokens: bfloat16 [1536, 4096], P(('gr', 'fs'), 'tp'), may hold values from -6 to 6
- route_ids: int32 [1536, 2], P(('gr', 'fs')), may hold values from 0 to 3, all different within a row; in each aligned block of 192 rows (0 to 191, 192 to 383, ...) at most 192 rows name the same one
- route_logits: float32 [1536, 2], P(('gr', 'fs')), may hold values from -6 to 6
- gain: float32 [4096], P(('gr', 'fs')), may hold values from 0.1 to 1.9
- gate_master: float32 [4, 4096, 2048], P(None, ('gr', 'fs'), 'tp'), may hold values from -6 to 6
- up_master: float32 [4, 4096, 2048], P(None, ('gr', 'fs'), 'tp'), may hold values from -6 to 6
- down_master: float32 [4, 2048, 4096], P(None, ('gr', 'fs'), 'tp'), may hold values from -6 to 6
Outputs:
- gate_weight: bfloat16 [4, 4096, 2048], P('fs', None, 'tp')
- up_weight: bfloat16 [4, 4096, 2048], P('fs', None, 'tp')
- down_weight: bfloat16 [4, 2048, 4096], P('fs', 'tp')
- mixed_out: bfloat16 [1536, 4096], P(('gr', 'fs'), 'tp')
Inputs may be any that keep to these rules, and one draw needn't show every extreme that they name: `route_ids`: each row names 2 different experts; among the rows of one device no expert is named by more than 192 rows, a bound that some block reaches.
All inputs are finite; a program needn't handle non-finite values.
Results may differ from a plain program's by a relative error of at most 0.015.
Values may be sent and summed in bfloat16 or wider, within the bound.
A program may use at most 128 MiB of HBM per device.

v0:
```python
import jax
import jax.numpy as jnp
from jax import lax
from jax.sharding import PartitionSpec as P

EPS = 1e-06


def slot_tables(route_ids, experts, capacity):
    assign_count = route_ids.shape[0] * route_ids.shape[1]
    flattened = route_ids.reshape(assign_count)
    onehot = (flattened[:, None] == jnp.arange(experts, dtype=jnp.int32)[None, :]).astype(jnp.int32)
    earlier = jnp.cumsum(onehot, axis=0) - onehot
    slot_rank = jnp.sum(earlier * onehot, axis=1)
    position = flattened * capacity + slot_rank
    source = (
        jnp.full((experts * capacity,), assign_count, jnp.int32)
        .at[position]
        .set(jnp.arange(assign_count, dtype=jnp.int32))
    )
    return (position, source)


def fill_slots(normed, source, top_count, experts, capacity):
    token_total = normed.shape[0]
    padded = jnp.concatenate([normed, jnp.zeros((1, normed.shape[1]), normed.dtype)], axis=0)
    token_index = jnp.where(source < token_total * top_count, source // top_count, token_total)
    return padded[token_index].reshape(experts, capacity, normed.shape[1])


def body(tokens, route_ids, route_logits, gain, gate_master, up_master, down_master):
    experts = gate_master.shape[0]
    token_total = route_ids.shape[0]
    top_count = route_ids.shape[1]
    capacity = 2 * token_total * top_count // experts
    row_gain = gain[None, :, None]
    gate_cast = (gate_master * row_gain).astype(jnp.bfloat16)
    up_cast = (up_master * row_gain).astype(jnp.bfloat16)
    down_cast = down_master.astype(jnp.bfloat16)
    owner_gate, owner_up, owner_down = (
        lax.all_to_all(gate_cast, "fs", split_axis=0, concat_axis=1, tiled=True),
        lax.all_to_all(up_cast, "fs", split_axis=0, concat_axis=1, tiled=True),
        lax.all_to_all(down_cast, "fs", split_axis=0, concat_axis=1, tiled=True),
    )
    gate_full, up_full, down_full = (
        lax.all_gather(owner_gate, "gr", axis=1, tiled=True),
        lax.all_gather(owner_up, "gr", axis=1, tiled=True),
        lax.all_gather(owner_down, "gr", axis=1, tiled=True),
    )
    down_rows = lax.all_to_all(down_full, "tp", split_axis=1, concat_axis=2, tiled=True)
    sigmoid_vals = jax.nn.sigmoid(route_logits)
    shares = sigmoid_vals / jnp.sum(sigmoid_vals, axis=1, keepdims=True)
    position, source = slot_tables(route_ids, experts, capacity)
    model_width = gate_full.shape[1]
    full_rows = lax.all_gather(tokens, "tp", axis=1, tiled=True)
    float_rows = full_rows.astype(jnp.float32)
    normed = (
        float_rows * lax.rsqrt(jnp.mean(float_rows * float_rows, axis=1, keepdims=True) + EPS)
    ).astype(jnp.bfloat16)
    buffer = fill_slots(normed, source, top_count, experts, capacity)
    arrived = lax.all_to_all(buffer, "fs", split_axis=0, concat_axis=1, tiled=True)
    gate_sum = jnp.einsum("erd,edf->erf", arrived, gate_full, preferred_element_type=jnp.float32)
    up_sum = jnp.einsum("erd,edf->erf", arrived, up_full, preferred_element_type=jnp.float32)
    scale_in = model_width ** (-0.5)
    hidden = (jax.nn.silu(gate_sum * scale_in) * (up_sum * scale_in)).astype(jnp.bfloat16)
    partial_value = jnp.einsum(
        "erf,efd->erd", hidden, down_rows, preferred_element_type=jnp.float32
    )
    summed = lax.psum_scatter(
        partial_value.astype(jnp.bfloat16), "tp", scatter_dimension=2, tiled=True
    ).astype(jnp.float32)
    expert_out = (summed * down_full.shape[1] ** (-0.5)).astype(jnp.bfloat16)
    returned = lax.all_to_all(expert_out, "fs", split_axis=1, concat_axis=0, tiled=True)
    picked = returned.reshape(experts * capacity, returned.shape[2])[position].astype(jnp.float32)
    weighted = picked * shares.reshape(token_total * top_count)[:, None]
    mixed_out = jnp.sum(weighted.reshape(token_total, top_count, returned.shape[2]), axis=1).astype(
        jnp.bfloat16
    )
    return (gate_full, up_full, down_rows, mixed_out)


def solution(mesh):
    in_specs = (
        P(("gr", "fs"), "tp"),
        P(("gr", "fs"), None),
        P(("gr", "fs"), None),
        P(("gr", "fs")),
        P(None, ("gr", "fs"), "tp"),
        P(None, ("gr", "fs"), "tp"),
        P(None, ("gr", "fs"), "tp"),
    )
    out_specs = (
        P("fs", None, "tp"),
        P("fs", None, "tp"),
        P("fs", "tp", None),
        P(("gr", "fs"), "tp"),
    )
    return jax.shard_map(body, mesh=mesh, in_specs=in_specs, out_specs=out_specs, check_vma=False)
```

profile of v0, /device:TPU:0, one launch (start us, length us, event | category | flops | bytes accessed | tf_op | source)
XLA Modules:
  0.0 531.2 jit_solution(6687284316396528108)
XLA Ops:
  7.2 3.8 convert_element_type.50
  11.0 6.5 %all-to-all-start.2 = ((bf16[4,256,1024]{2,1,0:T(8,128)(2,1)}), bf16[4,256,1024]{2,1,0:T(8,128)(2,1)S(1)}, u32[]{:S(2)}, u32[]{:S(2)}) async-start(bf16[4,256,1024]{2,1,0:T(8,128)(2,1)} %convert_element_type.50), calls=%async_computation.2 | async-start | bytes 4194304 | tf_op jit(solution)/shard_map/all_to_all | solution.py:43
  17.5 6.8 %multiply_convert_fusion = (bf16[4,512,512]{2,1,0:T(8,128)(2,1)}, bf16[4,512,512]{2,1,0:T(8,128)(2,1)}) fusion(f32[4,512,512]{2,1,0:T(8,128)} %param.12, f32[512]{0:T(512)S(1)} %copy-done.5, f32[4,512,512]{2,1,0:T(8,128)} %param.11), kind=kLoop, calls=%fused_computation.9 | loop fusion | flops 4194304 | bytes 12584960 | tf_op jit(solution)/shard_map/convert_element_type | solution.py:38
  24.2 41.4 %all-to-all-done.2 = bf16[4,256,1024]{2,1,0:T(8,128)(2,1)S(1)} async-done(((bf16[4,256,1024]{2,1,0:T(8,128)(2,1)}), bf16[4,256,1024]{2,1,0:T(8,128)(2,1)S(1)}, u32[]{:S(2)}, u32[]{:S(2)}) %all-to-all-start.2) | async-done | bytes 2097184 | tf_op jit(solution)/shard_map/all_to_all | solution.py:43
  65.7 1.3 copy-done.1
  67.0 3.6 all-to-all-start.1
  70.7 0.7 all-gather.9.cloned.1.call-update
  71.4 47.0 %all-to-all-done.1 = bf16[4,512,512]{2,1,0:T(8,128)(2,1)S(1)} async-done(((bf16[4,512,512]{2,1,0:T(8,128)(2,1)}), bf16[4,512,512]{2,1,0:T(8,128)(2,1)S(1)}, u32[]{:S(2)}, u32[]{:S(2)}) %all-to-all-start.1) | async-done | bytes 2097184 | tf_op jit(solution)/shard_map/all_to_all | solution.py:42
  118.3 4.5 all-to-all-start
  122.8 0.7 all-gather.11.cloned.1.call-update
  123.6 8.2 %all-gather.9.cloned.1.call-done = bf16[1,2048,1024]{2,1,0:T(8,128)(2,1)} async-done(((bf16[1,1024,1024]{2,1,0:T(8,128)(2,1)}), bf16[1,2048,1024]{2,1,0:T(8,128)(2,1)}) %all-gather.9.cloned.1.call-update) | async-done | bytes 4194320 | tf_op jit(solution)/shard_map/all_gather | solution.py:48
  131.7 8.6 %copy.48 = bf16[1,2048,1024]{2,0,1:T(2,128)(2,1)} copy(bf16[1,2048,1024]{2,1,0:T(8,128)(2,1)} %all-gather.9.cloned.1.call-done) | data formatting | bytes 8388608 | tf_op jit(solution)/shard_map/all_gather | solution.py:48
  140.3 0.5 broadcast.121
  140.8 26.0 %reduce.4 = bf16[2048,1024]{1,0:T(8,128)(2,1)} reduce(bf16[2048,1,1024]{2,1,0:T(2,128)(2,1)} %bitcast.63, bf16[]{:T(256)} %broadcast.121), dimensions={1}, to_apply=%bitcast.59.reduce_sub_computation | reduce | bytes 8388610
  166.9 6.2 %reshape.164 = bf16[4,2,262144]{2,1,0:T(2,128)(2,1)} reshape(bf16[2048,1024]{1,0:T(8,128)(2,1)} %reduce.4) | data formatting | bytes 8388608
  173.1 5.0 all-to-all-start.3
  178.6 1.2 reduce-window.6
  179.8 0.2 slice_reduce_fusion
  180.6 2.9 scatter_custom_fusion
  183.6 1.8 fusion.5
  185.4 1.8 fusion.6
  187.4 5.7 %gather_fusion = bf16[768,4096]{1,0:T(8,128)(2,1)} fusion(bf16[193,4096]{1,0:T(8,128)(2,1)S(1)} %concatenate.3, s32[1024]{0:T(1024)S(1)} %pad_clamp_fusion.1), kind=kCustom, calls=%fused_computation | custom fusion | bytes 12585984 | tf_op jit(solution)/shard_map/gather | solution.py:28
  193.1 33.3 %all-to-all-done.3 = bf16[4,2,262144]{2,1,0:T(2,128)(2,1)} async-done(((bf16[4,2,262144]{2,1,0:T(2,128)(2,1)}), bf16[4,2,262144]{2,1,0:T(2,128)(2,1)}, u32[]{:S(2)}, u32[]{:S(2)}) %all-to-all-start.3) | async-done | bytes 4194336 | tf_op jit(solution)/shard_map/all_to_all | solution.py:50
  226.3 5.3 %all-to-all-start.4 = ((bf16[4,192,4096]{2,1,0:T(8,128)(2,1)}), bf16[4,192,4096]{2,1,0:T(8,128)(2,1)}, u32[]{:S(2)}, u32[]{:S(2)}) async-start(bf16[4,192,4096]{2,1,0:T(8,128)(2,1)} %bitcast.65), calls=%async_computation.4 | async-start | bytes 12582912 | tf_op jit(solution)/shard_map/all_to_all | solution.py:61
  231.7 0.7 all-gather.7.cloned.1.call-update
  232.4 0.5 all-gather.5.cloned.1.call-update
  233.2 7.4 %reshape.165 = bf16[2048,1,1024]{2,1,0:T(2,128)(2,1)} reshape(bf16[4,2,262144]{2,1,0:T(2,128)(2,1)} %all-to-all-done.3) | data formatting | bytes 8388608
  240.6 8.0 %copy.40 = bf16[1,2048,1024]{2,1,0:T(8,128)(2,1)} copy(bf16[1,2048,1024]{2,0,1:T(2,128)(2,1)} %bitcast.64) | data formatting | bytes 8388608
  248.6 6.2 %copy.32 = bf16[1,512,4,1024]{1,3,2,0:T(8,128)(2,1)} copy(bf16[1,512,4,1024]{3,1,2,0:T(8,128)(2,1)} %bitcast.66) | data formatting | bytes 8388608 | tf_op jit(solution)/shard_map/all_to_all | solution.py:50
  254.8 35.5 %all-gather.7.cloned.1.call-done = bf16[1,4096,512]{2,1,0:T(8,128)(2,1)} async-done(((bf16[1,2048,512]{2,1,0:T(8,128)(2,1)}), bf16[1,4096,512]{2,1,0:T(8,128)(2,1)}) %all-gather.7.cloned.1.call-update) | async-done | bytes 4194320 | tf_op jit(solution)/shard_map/all_gather | solution.py:47
  290.3 79.5 %all-to-all-done.4 = bf16[4,192,4096]{2,1,0:T(8,128)(2,1)} async-done(((bf16[4,192,4096]{2,1,0:T(8,128)(2,1)}), bf16[4,192,4096]{2,1,0:T(8,128)(2,1)}, u32[]{:S(2)}, u32[]{:S(2)}) %all-to-all-start.4) | async-done | bytes 6291488 | tf_op jit(solution)/shard_map/all_to_all | solution.py:61
  369.8 6.7 %fusion.1 = f32[768,512]{1,0:T(8,128)S(1)} fusion(bf16[768,4096]{1,0:T(8,128)(2,1)} %bitcast.7, bf16[1,4096,512]{2,1,0:T(8,128)(2,1)} %all-gather.7.cloned.1.call-done), kind=kOutput, calls=%fused_computation.5 | convolution fusion | flops 3221225472 | bytes 12058624 | tf_op jit(solution)/shard_map/erd,edf->erf/dot_general | solution.py:63
  376.6 13.5 %fusion = bf16[1,768,4096]{2,1,0:T(8,128)(2,1)} fusion(bf16[512,4096]{0,1:T(8,128)(2,1)} %bitcast.67, f32[768,512]{1,0:T(8,128)S(1)} %fusion.1, bf16[768,4096]{1,0:T(8,128)(2,1)} %bitcast.7, bf16[1,4096,512]{2,1,0:T(8,128)(2,1)} %all-gather.5.cloned.1.call-done), kind=kOutput, calls=%fused_computation.4 | convolution fusion | flops 6448742400 | bytes 22544384 | tf_op jit(solution)/shard_map/erf,efd->erd/dot_general | solution.py:66
  390.1 55.4 %reduce-scatter.2.cloned.1.call-done = bf16[1,768,1024]{2,1,0:T(8,128)(2,1)} async-done(((bf16[1,768,4096]{2,1,0:T(8,128)(2,1)}), bf16[1,768,1024]{2,1,0:T(8,128)(2,1)}) %reduce-scatter.2.cloned.1.call-update) | async-done | bytes 1572880 | tf_op jit(solution)/shard_map/reduce_scatter | solution.py:69
  445.5 1.8 multiply_convert_fusion.2
  447.3 2.4 copy.49
  449.8 11.3 %reduce.5 = bf16[768,1024]{1,0:T(8,128)(2,1)} reduce(bf16[768,1,1024]{2,1,0:T(2,128)(2,1)S(1)} %bitcast.69, bf16[]{:T(256)} %broadcast.121), dimensions={1}, to_apply=%bitcast.60.reduce_sub_computation | reduce | bytes 3145730
  461.0 4.1 reshape.166
  465.1 4.6 all-to-all-start.5
  469.9 6.3 %copy.39 = bf16[1,512,4096]{2,1,0:T(8,128)(2,1)} copy(bf16[1,512,4096]{1,2,0:T(8,128)(2,1)} %bitcast.68) | data formatting | bytes 8388608
  476.3 30.3 %all-to-all-done.5 = bf16[4,2,98304]{2,1,0:T(2,128)(2,1)S(1)} async-done(((bf16[4,2,98304]{2,1,0:T(2,128)(2,1)}), bf16[4,2,98304]{2,1,0:T(2,128)(2,1)S(1)}, u32[]{:S(2)}, u32[]{:S(2)}) %all-to-all-start.5) | async-done | bytes 1572896 | tf_op jit(solution)/shard_map/all_to_all | solution.py:73
  506.5 2.8 reshape.167
  509.3 2.5 copy.47
  511.8 2.1 gather_fusion.1
  513.9 1.0 reshape.134
  514.9 2.8 multiply_reduce_fusion
  517.6 4.6 copy.52
  522.3 2.0 copy.53
  (40 shorter events, 1.8 us)
Async XLA Ops:
  11.0 6.5 %copy-start.5 = (f32[512]{0:T(512)S(1)}, f32[512]{0:T(512)}, u32[]{:S(2)}) copy-start(f32[512]{0:T(512)} %param.10) | copy-start | bytes 6148
  11.0 54.7 %all-to-all-start.2 = ((bf16[4,256,1024]{2,1,0:T(8,128)(2,1)}), bf16[4,256,1024]{2,1,0:T(8,128)(2,1)S(1)}, u32[]{:S(2)}, u32[]{:S(2)}) async-start(bf16[4,256,1024]{2,1,0:T(8,128)(2,1)} %convert_element_type.50), calls=%async_computation.2 | async-start | bytes 4194304 | tf_op jit(solution)/shard_map/all_to_all | solution.py:43
  65.7 1.3 copy-start.1
  67.0 51.3 %all-to-all-start.1 = ((bf16[4,512,512]{2,1,0:T(8,128)(2,1)}), bf16[4,512,512]{2,1,0:T(8,128)(2,1)S(1)}, u32[]{:S(2)}, u32[]{:S(2)}) async-start(bf16[4,512,512]{2,1,0:T(8,128)(2,1)} %get-tuple-element.16), calls=%async_computation.1 | async-start | bytes 4194304 | tf_op jit(solution)/shard_map/all_to_all | solution.py:42
  70.6 61.1 %all-gather.9.cloned.1.call-start = ((), (), s32[]{:S(2)}) async-start(), calls=%async_computation.9 | async-start | bytes 6291456 | tf_op jit(solution)/shard_map/all_gather | solution.py:48
  118.3 22.0 %copy-start = (bf16[4,512,512]{2,1,0:T(8,128)(2,1)}, bf16[4,512,512]{2,1,0:T(8,128)(2,1)S(1)}, u32[]{:S(2)}) copy-start(bf16[4,512,512]{2,1,0:T(8,128)(2,1)S(1)} %all-to-all-done.1) | copy-start | bytes 6291460
  118.3 54.7 %all-to-all-start = ((bf16[4,512,512]{2,1,0:T(8,128)(2,1)}), bf16[4,512,512]{2,1,0:T(8,128)(2,1)}, u32[]{:S(2)}, u32[]{:S(2)}) async-start(bf16[4,512,512]{2,1,0:T(8,128)(2,1)} %get-tuple-element.17), calls=%async_computation | async-start | bytes 4194304 | tf_op jit(solution)/shard_map/all_to_all | solution.py:41
  122.8 60.8 %all-gather.11.cloned.1.call-start = ((), (), s32[]{:S(2)}) async-start(), calls=%async_computation.10 | async-start | bytes 1966080 | tf_op jit(solution)/shard_map/all_gather | solution.py:55
  173.1 5.1 copy-start.3
  173.1 53.3 %all-to-all-start.3 = ((bf16[4,2,262144]{2,1,0:T(2,128)(2,1)}), bf16[4,2,262144]{2,1,0:T(2,128)(2,1)}, u32[]{:S(2)}, u32[]{:S(2)}) async-start(bf16[4,2,262144]{2,1,0:T(2,128)(2,1)} %reshape.164), calls=%async_computation.3 | async-start | bytes 8388608 | tf_op jit(solution)/shard_map/all_to_all | solution.py:50
  226.3 143.4 %all-to-all-start.4 = ((bf16[4,192,4096]{2,1,0:T(8,128)(2,1)}), bf16[4,192,4096]{2,1,0:T(8,128)(2,1)}, u32[]{:S(2)}, u32[]{:S(2)}) async-start(bf16[4,192,4096]{2,1,0:T(8,128)(2,1)} %bitcast.65), calls=%async_computation.4 | async-start | bytes 12582912 | tf_op jit(solution)/shard_map/all_to_all | solution.py:61
  231.7 58.6 %all-gather.7.cloned.1.call-start = ((), (), s32[]{:S(2)}) async-start(), calls=%async_computation.8 | async-start | bytes 6291456 | tf_op jit(solution)/shard_map/all_gather | solution.py:47
  232.4 144.1 %all-gather.5.cloned.1.call-start = ((), (), s32[]{:S(2)}) async-start(), calls=%async_computation.7 | async-start | bytes 6291456 | tf_op jit(solution)/shard_map/all_gather | solution.py:46
  233.0 212.6 %reduce-scatter.2.cloned.1.call-start = ((), (), s32[]{:S(2)}) async-start(), calls=%async_computation.11 | async-start | bytes 7864320 | tf_op jit(solution)/shard_map/reduce_scatter | solution.py:69
  461.0 8.7 %copy-start.4 = (f32[192,2]{0,1:T(2,128)S(1)}, f32[192,2]{0,1:T(2,128)}, u32[]{:S(2)}) copy-start(f32[192,2]{0,1:T(2,128)} %param.9) | copy-start | bytes 4612
  465.1 41.4 %all-to-all-start.5 = ((bf16[4,2,98304]{2,1,0:T(2,128)(2,1)}), bf16[4,2,98304]{2,1,0:T(2,128)(2,1)S(1)}, u32[]{:S(2)}, u32[]{:S(2)}) async-start(bf16[4,2,98304]{2,1,0:T(2,128)(2,1)} %reshape.166), calls=%async_computation.6 | async-start | bytes 3145728 | tf_op jit(solution)/shard_map/all_to_all | solution.py:73
  517.6 4.6 copy-start.2
Sparse Core Ops, SparseCore 0:
  73.5 58.1 all-gather.8
  133.3 19.6 all-gather.10
  234.0 56.2 all-gather.6
  291.7 56.7 all-gather.4
  390.2 55.2 reduce-scatter.1
where the time goes:
time: 540 us; the launch traced here: 531 us
  waiting for transfers between devices  333 us (62%)
  local copies, waits for them, and re-layouts  75.8 us (14%)
  other arithmetic  57.6 us (11%)
  starting transfers between devices  29.9 us (6%)
  matrix products  20.2 us (4%)
  between operations  14.4 us (3%)
    all_to_all x1, waiting for transfers between devices, body(): lax.all_to_all(buffer, 'fs', split_axis=0, concat_axis=1, tiled=True)  79.5 us
    reduce_scatter x1, waiting for transfers between devices, body(): lax.psum_scatter(partial_value.astype(jnp.bfloat16), 'tp', scatter_dimens...  55.4 us
    all_to_all x1, waiting for transfers between devices, body(): lax.all_to_all(up_cast, 'fs', split_axis=0, concat_axis=1, tiled=True)  47 us
    unnamed x23, local copies, waits for them, and re-layouts  45.9 us
    all_to_all x1, waiting for transfers between devices, body(): lax.all_to_all(down_cast, 'fs', split_axis=0, concat_axis=1, tiled=True)  41.4 us
    unnamed x3, other arithmetic  37.3 us
    all_gather x1, waiting for transfers between devices, body(): lax.all_gather(owner_up, 'gr', axis=1, tiled=True)  35.5 us
    all_to_all x1, waiting for transfers between devices, body(): lax.all_to_all(down_full, 'tp', split_axis=1, concat_axis=2, tiled=True)  33.3 us
  transfers between devices with their start and end apart: 11, of which 8 were waited for; matrix products, arithmetic and copies ran while one was open for 18% of the time, Pallas kernels for 0%

commit v1 on v0

v1 whole, which is shorter than its diff:
```python
import functools

import jax
import jax.numpy as jnp
from jax import lax
from jax.experimental import pallas as pl
from jax.experimental.pallas import tpu as pltpu
from jax.sharding import PartitionSpec as P

EPS = 1e-06
MESH = pl.DeviceIdType.MESH


def greet(sizes):
    barrier = pltpu.get_barrier_semaphore()
    count = 0
    for name, size in sizes:
        me = lax.axis_index(name)
        for off in range(1, size):
            other = lax.rem(me + off, size)
            pl.semaphore_signal(barrier, inc=1, device_id={name: other}, device_id_type=MESH)
            count += 1
    pl.semaphore_wait(barrier, count)


def step_order(n_fs):
    return sorted(range(1, n_fs), key=lambda s: (-min(s, n_fs - s), s))


def spread(n_gr, n_fs, src, dst, zs, zr, xs, xr, ls):
    g, f = lax.axis_index("gr"), lax.axis_index("fs")
    own = dst.shape[0]
    rows = src.shape[1]

    def place(gg, s):
        return dst.at[:, pl.ds(pl.multiple_of((gg * n_fs + s) * rows, rows), rows), :]

    def piece(e):
        return src.at[pl.ds(e * own, own)]

    sends = {}
    for step in step_order(n_fs):
        p = lax.rem(f + step, n_fs)
        copy = pltpu.make_async_remote_copy(
            src_ref=piece(p),
            dst_ref=place(g, f),
            send_sem=zs.at[step],
            recv_sem=zr.at[step],
            device_id={"fs": p},
            device_id_type=MESH,
        )
        copy.start()
        sends[step] = copy
    local = pltpu.make_async_copy(piece(f), place(g, f), ls)
    local.start()

    forwards = {}

    def forward(step):
        s = lax.rem(f + n_fs - step, n_fs)
        for o in range(1, n_gr):
            copy = pltpu.make_async_remote_copy(
                src_ref=piece(f) if step == 0 else place(g, s),
                dst_ref=place(g, s),
                send_sem=xs.at[o - 1, step],
                recv_sem=xr.at[o - 1, step],
                device_id={"gr": lax.rem(g + o, n_gr)},
                device_id_type=MESH,
            )
            copy.start()
            forwards[o, step] = copy

    forward(0)
    return sends, local, forward, forwards


def pair_kernel(n_gr, n_fs, a, b, a_out, b_out, zs, zr, xs, xr, ls):
    greet((("gr", n_gr), ("fs", n_fs)))
    states = [
        spread(n_gr, n_fs, src, dst, zs.at[m], zr.at[m], xs.at[m], xr.at[m], ls.at[m])
        for m, (src, dst) in enumerate(((a, a_out), (b, b_out)))
    ]
    for sends, _, forward, _ in states:
        for step in step_order(n_fs):
            sends[step].wait_recv()
            forward(step)
    for sends, local, _, forwards in states:
        local.wait()
        for copy in sends.values():
            copy.wait_send()
        for copy in forwards.values():
            copy.wait_send()
            copy.wait_recv()


def down_kernel(n_gr, n_fs, n_tp, a, cols_out, rows_out, held, zs, zr, xs, xr, ls, ys, yr, ks):
    greet((("gr", n_gr), ("fs", n_fs), ("tp", n_tp)))
    g, f, t = lax.axis_index("gr"), lax.axis_index("fs"), lax.axis_index("tp")
    rows, width = a.shape[1], a.shape[2]
    per = n_gr * n_fs // n_tp
    sends, local, forward, forwards = spread(n_gr, n_fs, a, held, zs, zr, xs, xr, ls)
    handed = []

    def hand(o, step):
        b = lax.rem(g + n_gr - o, n_gr) * n_fs + lax.rem(f + n_fs - step, n_fs)
        j, i = b // per, lax.rem(b, per)
        src = held.at[:, pl.ds(pl.multiple_of(b * rows, rows), rows), :]
        dst = rows_out.at[
            :,
            pl.ds(pl.multiple_of(i * rows, rows), rows),
            pl.ds(pl.multiple_of(t * width, width), width),
        ]
        stay = pltpu.make_async_copy(src, dst, ks.at[o, step])
        go = pltpu.make_async_remote_copy(
            src_ref=src,
            dst_ref=dst,
            send_sem=ys.at[o, step],
            recv_sem=yr.at[lax.rem(j + n_tp - t, n_tp), i],
            device_id={"tp": j},
            device_id_type=MESH,
        )

        @pl.when(j == t)
        def _():
            stay.start()

        @pl.when(j != t)
        def _():
            go.start()

        handed.append((j, stay, go))

    local.wait()
    hand(0, 0)
    for step in step_order(n_fs):
        sends[step].wait_recv()
        forward(step)
        hand(0, step)
    for (o, step), copy in forwards.items():
        copy.wait_recv()
        hand(o, step)
    whole = pltpu.make_async_copy(held, cols_out, ls)
    whole.start()
    for copy in sends.values():
        copy.wait_send()
    for copy in forwards.values():
        copy.wait_send()
    for j, stay, go in handed:

        @pl.when(j == t)
        def _():
            stay.wait()

        @pl.when(j != t)
        def _():
            go.wait_send()

    for k in range(1, n_tp):
        source = lax.rem(t + n_tp - k, n_tp)
        for i in range(per):
            pltpu.make_async_remote_copy(
                src_ref=held.at[:, pl.ds(i * rows, rows), :],
                dst_ref=rows_out.at[
                    :, pl.ds(i * rows, rows), pl.ds(pl.multiple_of(source * width, width), width)
                ],
                send_sem=ys.at[0, 0],
                recv_sem=yr.at[k, i],
                device_id={"tp": source},
                device_id_type=MESH,
            ).wait_recv()
    whole.wait()


def exchange_pair(a, b, n_gr, n_fs):
    experts, rows, width = a.shape
    out = jax.ShapeDtypeStruct((experts // n_fs, n_gr * n_fs * rows, width), a.dtype)
    dma = pltpu.SemaphoreType.DMA
    size = a.size * 2
    return pl.pallas_call(
        functools.partial(pair_kernel, n_gr, n_fs),
        out_shape=(out, out),
        in_specs=[pl.BlockSpec(memory_space=pltpu.VMEM)] * 2,
        out_specs=(pl.BlockSpec(memory_space=pl.ANY),) * 2,
        scratch_shapes=[
            dma((2, n_fs)),
            dma((2, n_fs)),
            dma((2, n_gr - 1, n_fs)),
            dma((2, n_gr - 1, n_fs)),
            dma((2,)),
        ],
        compiler_params=pltpu.CompilerParams(collective_id=1, has_side_effects=True),
        cost_estimate=pl.CostEstimate(flops=0, bytes_accessed=size * 80, transcendentals=0),
        name="pair_exchange",
    )(a, b)


def exchange_down(a, n_gr, n_fs, n_tp):
    experts, rows, width = a.shape
    own = experts // n_fs
    full = n_gr * n_fs * rows
    dma = pltpu.SemaphoreType.DMA
    size = a.size * 2
    return pl.pallas_call(
        functools.partial(down_kernel, n_gr, n_fs, n_tp),
        out_shape=(
            jax.ShapeDtypeStruct((own, full, width), a.dtype),
            jax.ShapeDtypeStruct((own, full // n_tp, width * n_tp), a.dtype),
        ),
        in_specs=[pl.BlockSpec(memory_space=pltpu.VMEM)],
        out_specs=(pl.BlockSpec(memory_space=pl.ANY),) * 2,
        scratch_shapes=[
            pltpu.VMEM((own, full, width), a.dtype),
            dma((n_fs,)),
            dma((n_fs,)),
            dma((n_gr - 1, n_fs)),
            dma((n_gr - 1, n_fs)),
            dma(()),
            dma((n_gr, n_fs)),
            dma((n_tp, n_gr * n_fs // n_tp)),
            dma((n_gr, n_fs)),
        ],
        compiler_params=pltpu.CompilerParams(collective_id=2, has_side_effects=True),
        cost_estimate=pl.CostEstimate(flops=0, bytes_accessed=size * 40, transcendentals=0),
        name="down_exchange",
    )(a)


def body(n_gr, n_fs, n_tp, tokens, route_ids, route_logits, gain, gate_master, up_master, down_master):
    experts = gate_master.shape[0]
    own = experts // n_fs
    model_width = gate_master.shape[1] * n_gr * n_fs
    hidden_width = gate_master.shape[2] * n_tp
    row_gain = gain[None, :, None]
    gate_cast = (gate_master * row_gain).astype(jnp.bfloat16)
    up_cast = (up_master * row_gain).astype(jnp.bfloat16)
    down_cast = down_master.astype(jnp.bfloat16)

    float_rows = tokens.astype(jnp.float32)
    squares = lax.psum(jnp.sum(float_rows * float_rows, axis=1, keepdims=True), "tp")
    normed = (float_rows * lax.rsqrt(squares / model_width + EPS)).astype(jnp.bfloat16)
    group = lax.all_gather(normed, "fs", axis=0, tiled=True)
    blocks = lax.all_gather(group, "tp", axis=0)

    sigmoid_vals = jax.nn.sigmoid(route_logits)
    shares = sigmoid_vals / jnp.sum(sigmoid_vals, axis=1, keepdims=True)
    chosen = route_ids[:, :, None] == jnp.arange(experts, dtype=jnp.int32)[None, None, :]
    weights = jnp.sum(jnp.where(chosen, shares[:, :, None], 0.0), axis=1)
    all_weights = lax.all_gather(weights, "fs", axis=0, tiled=True)

    gate_full, up_full = exchange_pair(gate_cast, up_cast, n_gr, n_fs)
    width = tokens.shape[1]
    scale_in = model_width ** (-0.5)

    def project(matrix):
        return sum(
            jnp.dot(
                blocks[j],
                matrix[j * width : (j + 1) * width],
                preferred_element_type=jnp.float32,
            )
            for j in range(n_tp)
        )

    hidden = []
    for e in range(own):
        gate_value = project(gate_full[e]) * scale_in
        up_value = project(up_full[e]) * scale_in
        hidden.append((jax.nn.silu(gate_value) * up_value).astype(jnp.bfloat16))
    hidden = jnp.stack(hidden)
    down_cast, hidden = lax.optimization_barrier((down_cast, hidden))
    all_hidden = lax.all_gather(hidden, "tp", axis=0)
    down_cols, down_rows = exchange_down(down_cast, n_gr, n_fs, n_tp)

    part = hidden.shape[2]
    first = lax.axis_index("fs") * own
    total = 0.0
    for e in range(own):
        summed = sum(
            jnp.dot(
                all_hidden[j, e],
                down_cols[e, j * part : (j + 1) * part],
                preferred_element_type=jnp.float32,
            )
            for j in range(n_tp)
        )
        share = lax.dynamic_slice_in_dim(all_weights, first + e, 1, axis=1)
        total = total + summed * hidden_width ** (-0.5) * share
    mixed_out = lax.psum_scatter(
        total.astype(jnp.bfloat16), "fs", scatter_dimension=0, tiled=True
    )
    return (gate_full, up_full, down_rows, mixed_out)


def solution(mesh):
    in_specs = (
        P(("gr", "fs"), "tp"),
        P(("gr", "fs"), None),
        P(("gr", "fs"), None),
        P(("gr", "fs")),
        P(None, ("gr", "fs"), "tp"),
        P(None, ("gr", "fs"), "tp"),
        P(None, ("gr", "fs"), "tp"),
    )
    out_specs = (
        P("fs", None, "tp"),
        P("fs", None, "tp"),
        P("fs", "tp", None),
        P(("gr", "fs"), "tp"),
    )
    sizes = (mesh.shape["gr"], mesh.shape["fs"], mesh.shape["tp"])
    return jax.shard_map(
        functools.partial(body, *sizes), mesh=mesh, in_specs=in_specs, out_specs=out_specs, check_vma=False
    )
```

time: 540 us -> 368 us (0.68); the launches traced: 531 us -> 368 us
  waiting for transfers between devices: 333 us -> 82.3 us
  Pallas kernels: 0 us -> 204 us
  local copies, waits for them, and re-layouts: 75.8 us -> 11.9 us
  other arithmetic: 57.6 us -> 12.6 us
  starting transfers between devices: 29.9 us -> 0.16 us
  blocking collectives: 0 us -> 21.8 us
    all_to_all x6 -> x0, waiting for transfers between devices: 231 us -> none  [the longest x1 79.5 us: body(): lax.all_to_all(buffer, 'fs', split_axis=0, concat_axis=1, tiled=True)]
    pallas_call x0 -> x2, Pallas kernels: none -> 204 us  [the longest x1 120 us: exchange_pair(): pl.pallas_call(functools.partial(pair_kernel, n_gr, n_fs), out_shape=(out...]
    unnamed x3 -> x0, other arithmetic: 37.3 us -> none
    unnamed x23 -> x26, local copies, waits for them, and re-layouts: 45.9 us -> 11.9 us
    all_to_all x6 -> x0, starting transfers between devices: 29.5 us -> none  [the longest x1 6.48 us: body(): lax.all_to_all(down_cast, 'fs', split_axis=0, concat_axis=1, tiled=True)]
    all_gather x0 -> x1, blocking collectives: none -> 13.4 us  [body(): all_weights = lax.all_gather(weights, 'fs', axis=0, tiled=True)]
    reduce_scatter x1, waiting for transfers between devices: 55.4 us -> 44.8 us  [body(): lax.psum_scatter(total.astype(jnp.bfloat16), 'fs', scatter_dimension=0, t...]
    all_gather x1, local copies, waits for them, and re-layouts: 8.61 us -> 0.01 us  [body(): all_weights = lax.all_gather(weights, 'fs', axis=0, tiled=True)]
  transfers between devices with their start and end apart: 11 -> 4, of which waited for: 8 -> 2; matrix products, arithmetic and copies ran while one was open for 18% -> 3% of each run, Pallas kernels for 0% -> 55%
where the time goes in v1:
time: 368 us
  Pallas kernels  204 us (55%)
  waiting for transfers between devices  82.3 us (22%)
  blocking collectives  21.8 us (6%)
  matrix products  21.3 us (6%)
  between operations  14 us (4%)
  other arithmetic  12.6 us (3%)
  local copies, waits for them, and re-layouts  11.9 us (3%)
    pallas_call x1, Pallas kernels, exchange_pair(): pl.pallas_call(functools.partial(pair_kernel, n_gr, n_fs), out_shape=(out...  120 us
    pallas_call x1, Pallas kernels, exchange_down(): pl.pallas_call(functools.partial(down_kernel, n_gr, n_fs, n_tp), out_shap...  83.9 us
    reduce_scatter x1, waiting for transfers between devices, body(): lax.psum_scatter(total.astype(jnp.bfloat16), 'fs', scatter_dimension=0, t...  44.8 us
    all_gather x1, waiting for transfers between devices, body(): group = lax.all_gather(normed, 'fs', axis=0, tiled=True)  37.4 us
    all_gather x1, blocking collectives, body(): all_weights = lax.all_gather(weights, 'fs', axis=0, tiled=True)  13.4 us
    dot_general x8, matrix products, project(): jnp.dot(blocks[j], matrix[j * width:(j + 1) * width], preferred_element_t...  13.2 us
    unnamed x26, local copies, waits for them, and re-layouts  11.9 us
    psum x1, blocking collectives, body(): lax.psum(jnp.sum(float_rows * float_rows, axis=1, keepdims=True), 'tp')  8.39 us
  transfers between devices with their start and end apart: 4, of which 2 were waited for; matrix products, arithmetic and copies ran while one was open for 3% of the time, Pallas kernels for 55%

profile of v1, /device:TPU:0, one launch (start us, length us, event | category | flops | bytes accessed | tf_op | source)
XLA Modules:
  0.0 367.6 jit_solution(12837313132108912417)
XLA Ops:
  7.2 0.0 all-gather.7.cloned.1.call-start
  7.2 1.2 fusion.45
  8.4 8.4 %psum.7 = f32[192,1]{0,1:T(1,128)S(1)} all-reduce(f32[192,1]{0,1:T(1,128)S(1)} %bitcast.57), channel_id=1, replica_groups=mesh['gr'=2,'fs'=4,'tp'=4] {'tp'}, use_global_device_ids=true, to_apply=%region_1.0 | all-reduce | flops 192 | bytes 1536 | tf_op jit(solution)/shard_map/psum | solution.py:239
  16.8 1.9 fusion.46
  18.6 0.0 all-gather.7.cloned.1.call-update
  18.7 0.0 all-gather.9.cloned.1.call-start
  18.7 37.4 %all-gather.7.cloned.1.call-done = bf16[768,1024]{1,0:T(8,128)(2,1)} async-done(((bf16[192,1024]{1,0:T(8,128)(2,1)}), bf16[768,1024]{1,0:T(8,128)(2,1)}) %all-gather.7.cloned.1.call-update) | async-done | bytes 1572880 | tf_op jit(solution)/shard_map/all_gather | solution.py:241
  56.1 0.0 all-gather.9.cloned.1.call-update
  56.2 0.0 copy-start.9
  56.2 0.0 all-gather.11.cloned.1.call-start
  56.2 0.0 copy-start.1
  56.2 4.0 %convert_element_type.23.a = bf16[4,256,1024]{2,1,0:T(8,128)(2,1)} convert(f32[4,256,1024]{2,1,0:T(8,128)} %param.13) | non-fusion elementwise | flops 1048576 | bytes 6291456 | tf_op jit(solution)/shard_map/convert_element_type | solution.py:236
  60.2 0.0 copy-done.9
  60.2 0.0 copy-done.1
  60.2 5.5 %multiply_convert_fusion = (bf16[4,512,512]{2,1,0:T(8,128)(2,1)}, bf16[4,512,512]{2,1,0:T(8,128)(2,1)}) fusion(f32[4,512,512]{2,1,0:T(8,128)S(1)} %copy-done.1, f32[512]{0:T(512)S(1)} %copy-done.9, f32[4,512,512]{2,1,0:T(8,128)} %param.11), kind=kLoop, calls=%fused_computation | loop fusion | flops 4194304 | bytes 12584960 | tf_op jit(solution)/shard_map/convert_element_type | solution.py:235
  65.8 119.7 %pair_exchange.1 = (bf16[1,4096,512]{2,1,0:T(8,128)(2,1)}, bf16[1,4096,512]{2,1,0:T(8,128)(2,1)}) custom-call(bf16[4,512,512]{2,1,0:T(8,128)(2,1)} %get-tuple-element.17.a, bf16[4,512,512]{2,1,0:T(8,128)(2,1)} %get-tuple-element.16.b), custom_call_target="tpu_custom_call" | custom-call | bytes 167772160 | tf_op jit(solution)/shard_map/pair_exchange/pallas_call | solution.py:179
  185.5 0.0 all-gather.9.cloned.1.call-done
  185.5 2.8 fusion
  188.3 0.1 copy-done.4
  188.5 3.1 fusion.3
  191.6 0.0 copy-done.10
  191.6 1.0 fusion.7
  192.6 1.0 fusion.11
  193.6 1.2 copy-done.2
  194.8 1.0 fusion.5
  195.8 1.0 fusion.9
  196.8 1.0 fusion.13
  197.7 0.0 copy-start.7
  197.7 0.0 copy-start.8
  197.8 2.4 fusion.15
  200.1 0.0 all-gather.11.cloned.1.call-update
  200.2 0.0 reduce-scatter.2.cloned.1.call-start
  200.3 13.4 %all-gather.2 = f32[4,192,4]{1,2,0:T(4,128)S(1)} all-gather(f32[1,192,4]{1,2,0:T(4,128)S(1)} %bitcast.55), channel_id=1, replica_groups=mesh['gr'=2,'fs'=4,'tp'=4] {'fs'}, dimensions={0}, use_global_device_ids=true | all-gather | bytes 15360 | tf_op jit(solution)/shard_map/all_gather | solution.py:248
  213.7 0.1 reshape.41
  213.8 83.9 %down_exchange.1 = (bf16[1,2048,1024]{2,1,0:T(8,128)(2,1)}, bf16[1,512,4096]{2,1,0:T(8,128)(2,1)}) custom-call(bf16[4,256,1024]{2,1,0:T(8,128)(2,1)} %convert_element_type.23.a), custom_call_target="tpu_custom_call" | custom-call | bytes 83886080 | tf_op jit(solution)/shard_map/down_exchange/pallas_call | solution.py:203
  297.7 0.0 all-gather.11.cloned.1.call-done
  297.8 2.6 fusion.19
  300.3 0.1 copy-done
  300.5 2.3 fusion.21
  302.7 0.0 copy-done.6
  302.8 1.0 fusion.23
  303.7 2.2 multiply_convert_fusion.2
  306.0 0.0 reduce-scatter.2.cloned.1.call-update
  306.0 44.8 %reduce-scatter.2.cloned.1.call-done = bf16[192,1024]{1,0:T(8,128)(2,1)} async-done(((bf16[768,1024]{1,0:T(8,128)(2,1)}), bf16[192,1024]{1,0:T(8,128)(2,1)}) %reduce-scatter.2.cloned.1.call-update) | async-done | bytes 393232 | tf_op jit(solution)/shard_map/reduce_scatter | solution.py:288
  350.8 4.6 %copy.24 = bf16[1,4096,512]{2,1,0:T(8,128)(2,1)} copy(bf16[1,4096,512]{2,1,0:T(8,128)(2,1)} %get-tuple-element.22) | data formatting | bytes 8388608
  355.4 2.1 copy.25
  357.5 1.6 copy-done.5
  359.1 2.0 copy.26
  (16 shorter events, 0.1 us)
Async XLA Ops:
  7.2 49.0 %all-gather.7.cloned.1.call-start = ((), (), s32[]{:S(2)}) async-start(), calls=%async_computation.1 | async-start | bytes 1966080 | tf_op jit(solution)/shard_map/all_gather | solution.py:241
  18.7 166.8 %all-gather.9.cloned.1.call-start = ((), (), s32[]{:S(2)}) async-start(), calls=%async_computation.3 | async-start | bytes 7864320 | tf_op jit(solution)/shard_map/all_gather | solution.py:242
  56.2 4.1 %copy-start.9 = (f32[512]{0:T(512)S(1)}, f32[512]{0:T(512)}, u32[]{:S(2)}) copy-start(f32[512]{0:T(512)} %param.10) | copy-start | bytes 6148
  56.2 241.6 %all-gather.11.cloned.1.call-start = ((), (), s32[]{:S(2)}) async-start(), calls=%async_computation.4 | async-start | bytes 3932160 | tf_op jit(solution)/shard_map/all_gather | solution.py:271
  56.2 4.0 %copy-start.1 = (f32[4,512,512]{2,1,0:T(8,128)S(1)}, f32[4,512,512]{2,1,0:T(8,128)}, u32[]{:S(2)}) copy-start(f32[4,512,512]{2,1,0:T(8,128)} %param.12) | copy-start | bytes 12582916
  185.5 3.0 copy-start.4
  185.5 6.1 %copy-start.10 = (bf16[3072,1024]{1,0:T(8,128)(2,1)S(1)}, bf16[3072,1024]{1,0:T(8,128)(2,1)}, u32[]{:S(2)}) copy-start(bf16[3072,1024]{1,0:T(8,128)(2,1)} %all-gather.9.cloned.1.call-done) | copy-start | bytes 18874372
  192.6 2.2 copy-start.2
  197.7 2.5 copy-start.7
  197.7 2.5 copy-start.8
  200.2 150.6 %reduce-scatter.2.cloned.1.call-start = ((), (), s32[]{:S(2)}) async-start(), calls=%async_computation.2 | async-start | bytes 1966080 | tf_op jit(solution)/shard_map/reduce_scatter | solution.py:288
  297.7 2.7 copy-start
  300.5 2.3 copy-start.6
  350.8 4.6 %copy-start.3 = (bf16[1,4096,512]{2,1,0:T(8,128)(2,1)S(1)}, bf16[1,4096,512]{2,1,0:T(8,128)(2,1)}, u32[]{:S(2)}) copy-start(bf16[1,4096,512]{2,1,0:T(8,128)(2,1)} %get-tuple-element.23) | copy-start | bytes 12582916
  355.4 3.7 %copy-start.5 = (bf16[1,512,4096]{2,1,0:T(8,128)(2,1)S(1)}, bf16[1,512,4096]{2,1,0:T(8,128)(2,1)}, u32[]{:S(2)}) copy-start(bf16[1,512,4096]{2,1,0:T(8,128)(2,1)} %get-tuple-element.24) | copy-start | bytes 12582916
Sparse Core Ops, SparseCore 0:
  18.8 37.3 all-gather.6
  57.7 45.2 all-gather.8
  200.3 34.7 all-gather.10
  306.1 44.6 reduce-scatter.1
